TPU v7x, 1024 devices: a whole 8x8x8 slice. The times are simulated.
1024 devices in a mesh: ep: 64 (over z, y), tp: 16 (over x, core).
Axes of the slice: x: 8, y: 8, z: 8, core: 2. Of those that a mesh axis runs over, the one named last changes fastest.
Arguments:
- tokens: bfloat16 [8192, 2048], P('ep', 'tp'), may hold values from -6 to 6
- norm_gain: bfloat16 [2048], P('tp'), may hold values from 0.099609375 to 1.8984375
- routes: int32 [8192, 2], P('ep'), may hold values from 0 to 63, as said below
- gate_weights: float32 [8192, 2], P('ep'), may hold values from 0.1 to 1
- w_gate: bfloat16 [64, 2048, 4096], P('ep', None, 'tp'), may hold values from -0.125 to 0.125
- w_up: bfloat16 [64, 2048, 4096], P('ep', None, 'tp'), may hold values from -0.125 to 0.125
- w_down: bfloat16 [64, 4096, 2048], P('ep', 'tp'), may hold values from -0.875 to 0.875
- out_gain: bfloat16 [2048], P('tp'), may hold values from 0.099609375 to 1.8984375
Outputs:
- mixed: bfloat16 [8192, 2048], P('ep', 'tp')
Inputs may be any that keep to these rules, and one draw needn't show every extreme that they name: `routes`: each row names 2 different experts of one group (their quotients by 8 agree). In each aligned block of 128 rows no expert is named by more than 8 rows, and in every block some expert is named by exactly 8 rows.
All inputs are finite; a program needn't handle non-finite values.
Results may differ from a plain program's by a relative error of at most 0.019.
Values may be sent and summed in bfloat16 or wider, within the bound.
A program may use at most 32 MiB of HBM per device.

v0:
```python
import jax
import jax.numpy as jnp
from jax import lax
from jax.sharding import PartitionSpec as P

epsilon = 1e-06


def turned_gather(arrays, axis, dims):
    turned = [jnp.moveaxis(a, dim, 0) for a, dim in zip(arrays, dims)]
    widths = [t[0].size for t in turned]
    both = jnp.concatenate([t.reshape(-1, w) for t, w in zip(turned, widths)], axis=1)
    result = lax.all_gather(both, axis, axis=0, tiled=True)
    parts = jnp.split(result, [sum(widths[:k]) for k in range(1, len(widths))], axis=1)
    return tuple(
        (
            jnp.moveaxis(b.reshape(-1, *t.shape[1:]), 0, dim)
            for b, t, dim in zip(parts, turned, dims)
        )
    )


def in_blocks(x, dim, size):
    lengths = x.shape
    parts = x.reshape(*lengths[:dim], size, lengths[dim] // size, *lengths[dim + 1 :])
    return jnp.moveaxis(parts, dim, 0)


def sum_at_owner(x, axis, dim):
    size = lax.axis_size(axis)
    parts = lax.all_to_all(in_blocks(x, dim, size), axis, 0, 0, tiled=True)
    return jnp.sum(parts.astype(jnp.float32), axis=0)


def copy_for_each(x, axis):
    size = lax.axis_size(axis)
    return lax.all_to_all(jnp.broadcast_to(x[None], (size, *x.shape)), axis, 0, 0, tiled=True)


def taken_together(x, axis):
    return copy_for_each(x, axis).sum(axis=0)


def shards(tokens, norm_gain, routes, gate_weights, w_gate, w_up, w_down, out_gain):
    tok_rows = tokens.shape[0]
    width_local = tokens.shape[1]
    full_width = width_local * lax.axis_size("tp")
    experts = lax.axis_size("ep")
    top_count = routes.shape[1]
    capacity = 2 * top_count * tok_rows // experts
    flat_ids = routes.reshape(-1)
    onehot = (flat_ids[:, None] == jnp.arange(experts, dtype=jnp.int32)[None, :]).astype(jnp.int32)
    before = jnp.cumsum(onehot, axis=0) - onehot
    slot_index = jnp.sum(before * onehot, axis=1)
    dest_index = flat_ids * capacity + slot_index
    dest_pairs = dest_index.reshape(tok_rows, top_count)
    places = jnp.arange(experts * capacity, dtype=jnp.int32)
    scatter_mat = jnp.any(dest_pairs[None, :, :] == places[:, None, None], axis=2).astype(
        jnp.bfloat16
    )
    gate_mat = w_gate[0]
    up_mat = w_up[0]
    full_rows, gain_all = turned_gather((tokens, norm_gain), "tp", (1, 0))
    x_float = full_rows.astype(jnp.float32)
    scale_in = lax.rsqrt(jnp.mean(x_float * x_float, axis=1, keepdims=True) + epsilon)
    normed = (x_float * scale_in * gain_all.astype(jnp.float32)).astype(jnp.bfloat16)
    outgoing = jnp.dot(scatter_mat, normed, preferred_element_type=jnp.float32).astype(jnp.bfloat16)
    arrived = lax.all_to_all(outgoing, "ep", split_axis=0, concat_axis=0, tiled=True)
    gate_sum = jnp.dot(arrived, gate_mat, preferred_element_type=jnp.float32)
    up_sum = jnp.dot(arrived, up_mat, preferred_element_type=jnp.float32)
    hidden = (jax.nn.silu(gate_sum) * up_sum).astype(jnp.bfloat16)
    down_mat = w_down[0]
    summed = sum_at_owner(
        lax.dot_general(
            down_mat, hidden, (((0,), (1,)), ((), ())), preferred_element_type=jnp.float32
        ).astype(jnp.bfloat16),
        "tp",
        0,
    )
    expert_out = summed.astype(jnp.bfloat16)
    came_back = lax.all_to_all(expert_out, "ep", split_axis=1, concat_axis=1, tiled=True)
    picked = (
        jnp.take(came_back, dest_index, axis=1)
        .astype(jnp.float32)
        .reshape(width_local, tok_rows, top_count)
    )
    combined = jnp.sum(picked * gate_weights[None, :, :], axis=2).T
    out_sums = taken_together(jnp.sum(combined * combined, axis=1), "tp")
    scale_out = lax.rsqrt(out_sums / full_width + epsilon)
    return (combined * scale_out[:, None] * out_gain.astype(jnp.float32)).astype(jnp.bfloat16)


def solution(mesh):
    placed = (
        P("ep", "tp"),
        P("tp"),
        P("ep", None),
        P("ep", None),
        P("ep", None, "tp"),
        P("ep", None, "tp"),
        P("ep", "tp", None),
        P("tp"),
    )
    return jax.shard_map(
        shards, mesh=mesh, in_specs=placed, out_specs=P("ep", "tp"), check_vma=False
    )
```

profile of v0, /device:TPU:1, one launch (start us, length us, event | category | flops | bytes accessed | tf_op | source)
XLA Modules:
  0.0 202.8 jit_solution(17752862404031483606)
XLA Ops:
  0.0 0.9 copy.38
  0.9 0.1 eq.39
  1.0 0.1 reshape.107
  1.2 0.8 pad_maximum_fusion
  1.9 29.8 %all_gather.3 = bf16[2048,129]{0,1:T(8,128)(2,1)S(1)} all-gather(bf16[128,129]{0,1:T(8,128)(2,1)S(1)} %pad_maximum_fusion), channel_id=1, replica_groups=mesh['ep'=64,'tp'=16] {'tp'}, dimensions={0}, use_global_device_ids=true | all-gather | bytes 561408 | tf_op jit(solution)/shard_map/all_gather | solution.py:13
  31.7 0.2 fusion.12
  31.9 0.6 reduce-window.6
  32.5 0.2 slice_reduce_fusion
  32.8 0.1 fusion.35
  32.9 0.1 reduce_sum.62
  33.1 0.7 compare_and_fusion
  33.9 0.8 fusion
  34.7 63.1 %all_to_all.35 = bf16[64,8,2048]{2,1,0:T(8,128)(2,1)S(1)} all-to-all(bf16[64,8,2048]{2,1,0:T(8,128)(2,1)S(1)} %fusion), channel_id=1, replica_groups=mesh['ep'=64,'tp'=16] {'ep'}, dimensions={0} | all-to-all | bytes 4194304 | tf_op jit(solution)/shard_map/all_to_all | solution.py:68
  97.8 1.5 fusion.3
  99.3 5.0 %fusion.5 = bf16[64,16,8,128]{3,2,1,0:T(8,128)(2,1)} fusion(bf16[1,256,2048]{2,1,0:T(8,128)(2,1)S(1)} %copy-done, bf16[64,8,2048]{2,1,0:T(8,128)(2,1)S(1)} %all_to_all.35, bf16[1,2048,256]{2,1,0:T(8,128)(2,1)} %param.13, f32[512,256]{1,0:T(8,128)} %fusion.3), kind=kOutput, calls=%fused_computation.9 | convolution fusion | flops 1075576832 | bytes 6815744 | tf_op jit(solution)/shard_map/dot_general | solution.py:74
  104.4 3.4 %copy.51 = bf16[64,16,8,128]{3,2,0,1:T(8,128)(2,1)} copy(bf16[64,16,8,128]{3,2,1,0:T(8,128)(2,1)} %fusion.5) | data formatting | bytes 4194304 | tf_op jit(solution)/shard_map/reshape | solution.py:25
  107.8 8.2 %all-to-all-start.1 = ((bf16[16,128,512]{1,2,0:T(8,128)(2,1)}), bf16[16,128,512]{1,2,0:T(8,128)(2,1)S(1)}, u32[]{:S(2)}, u32[]{:S(2)}) async-start(bf16[16,128,512]{1,2,0:T(8,128)(2,1)} %bitcast.63), calls=%async_computation.1 | async-start | bytes 4194304 | tf_op jit(solution)/shard_map/all_to_all | solution.py:31
  116.0 0.1 copy.44
  116.2 0.1 mul.93
  116.3 0.1 copy.42
  116.5 0.1 copy.45
  116.6 48.5 %all-to-all-done.1 = bf16[16,128,512]{1,2,0:T(8,128)(2,1)S(1)} async-done(((bf16[16,128,512]{1,2,0:T(8,128)(2,1)}), bf16[16,128,512]{1,2,0:T(8,128)(2,1)S(1)}, u32[]{:S(2)}, u32[]{:S(2)}) %all-to-all-start.1) | async-done | bytes 2097184 | tf_op jit(solution)/shard_map/all_to_all | solution.py:31
  165.1 0.9 reduce_sum.64
  166.0 9.2 %all-to-all-start.2 = ((bf16[128,64,8]{0,2,1:T(8,128)(2,1)}), bf16[128,64,8]{0,2,1:T(8,128)(2,1)S(1)}, u32[]{:S(2)}, u32[]{:S(2)}) async-start(bf16[128,64,8]{0,2,1:T(8,128)(2,1)} %bitcast.10), calls=%async_computation.2 | async-start | bytes 262144 | tf_op jit(solution)/shard_map/all_to_all | solution.py:81
  175.2 11.5 %all-to-all-done.2 = bf16[128,64,8]{0,2,1:T(8,128)(2,1)S(1)} async-done(((bf16[128,64,8]{0,2,1:T(8,128)(2,1)}), bf16[128,64,8]{0,2,1:T(8,128)(2,1)S(1)}, u32[]{:S(2)}, u32[]{:S(2)}) %all-to-all-start.2) | async-done | bytes 131104 | tf_op jit(solution)/shard_map/all_to_all | solution.py:81
  186.8 0.9 gather_fusion
  187.6 0.3 multiply_reduce_fusion
  188.0 0.1 multiply_reduce_fusion.1
  188.1 0.6 broadcast_in_dim.14
  188.7 6.4 %all-to-all-start.3 = ((f32[16,1,128]{2,1,0:T(1,128)}), f32[16,1,128]{2,1,0:T(1,128)S(1)}, u32[]{:S(2)}, u32[]{:S(2)}) async-start(f32[16,1,128]{2,1,0:T(1,128)} %broadcast_in_dim.14), calls=%async_computation.3 | async-start | bytes 16384 | tf_op jit(solution)/shard_map/all_to_all | solution.py:37
  195.1 7.0 %all-to-all-done.3 = f32[16,1,128]{2,1,0:T(1,128)S(1)} async-done(((f32[16,1,128]{2,1,0:T(1,128)}), f32[16,1,128]{2,1,0:T(1,128)S(1)}, u32[]{:S(2)}, u32[]{:S(2)}) %all-to-all-start.3) | async-done | bytes 8224 | tf_op jit(solution)/shard_map/all_to_all | solution.py:37
  202.1 0.7 fusion.37
  (23 shorter events, 0.2 us)
Async XLA Ops:
  0.0 99.3 %copy-start = (bf16[1,256,2048]{2,1,0:T(8,128)(2,1)S(1)}, bf16[1,256,2048]{2,1,0:T(8,128)(2,1)}, u32[]{:S(2)}) copy-start(bf16[1,256,2048]{2,1,0:T(8,128)(2,1)} %param.14) | copy-start | bytes 3145732
  34.7 63.2 %copy-start.3 = (bf16[1,2048,256]{2,1,0:T(8,128)(2,1)S(1)}, bf16[1,2048,256]{2,1,0:T(8,128)(2,1)}, u32[]{:S(2)}) copy-start(bf16[1,2048,256]{2,1,0:T(8,128)(2,1)} %param.12) | copy-start | bytes 3145732
  107.8 8.2 %copy-start.1 = (s32[128,2]{0,1:T(2,128)S(1)}, s32[128,2]{0,1:T(2,128)}, u32[]{:S(2)}) copy-start(s32[128,2]{0,1:T(2,128)} %param.10) | copy-start | bytes 3076
  107.8 8.7 %copy-start.2 = (f32[128,2]{0,1:T(2,128)S(1)}, f32[128,2]{0,1:T(2,128)}, u32[]{:S(2)}) copy-start(f32[128,2]{0,1:T(2,128)} %param.11) | copy-start | bytes 3076
  107.8 57.3 %all-to-all-start.1 = ((bf16[16,128,512]{1,2,0:T(8,128)(2,1)}), bf16[16,128,512]{1,2,0:T(8,128)(2,1)S(1)}, u32[]{:S(2)}, u32[]{:S(2)}) async-start(bf16[16,128,512]{1,2,0:T(8,128)(2,1)} %bitcast.63), calls=%async_computation.1 | async-start | bytes 4194304 | tf_op jit(solution)/shard_map/all_to_all | solution.py:31
  116.0 79.1 %copy-start.4 = (bf16[128]{0:T(256)(128)(2,1)S(1)}, bf16[128]{0:T(256)(128)(2,1)}, u32[]{:S(2)}) copy-start(bf16[128]{0:T(256)(128)(2,1)} %param.15) | copy-start | bytes 772
  166.0 20.8 %all-to-all-start.2 = ((bf16[128,64,8]{0,2,1:T(8,128)(2,1)}), bf16[128,64,8]{0,2,1:T(8,128)(2,1)S(1)}, u32[]{:S(2)}, u32[]{:S(2)}) async-start(bf16[128,64,8]{0,2,1:T(8,128)(2,1)} %bitcast.10), calls=%async_computation.2 | async-start | bytes 262144 | tf_op jit(solution)/shard_map/all_to_all | solution.py:81
  188.7 13.4 %all-to-all-start.3 = ((f32[16,1,128]{2,1,0:T(1,128)}), f32[16,1,128]{2,1,0:T(1,128)S(1)}, u32[]{:S(2)}, u32[]{:S(2)}) async-start(f32[16,1,128]{2,1,0:T(1,128)} %broadcast_in_dim.14), calls=%async_computation.3 | async-start | bytes 16384 | tf_op jit(solution)/shard_map/all_to_all | solution.py:37
where the time goes:
time: 203 us
  blocking collectives  92.9 us (46%)
  waiting for transfers between devices  67 us (33%)
  starting transfers between devices  23.8 us (12%)
  matrix products  7.33 us (4%)
  local copies, waits for them, and re-layouts  6.96 us (3%)
  other arithmetic  4.66 us (2%)
    all_to_all x1, blocking collectives, shards(): lax.all_to_all(outgoing, 'ep', split_axis=0, concat_axis=0, tiled=True)  63.1 us
    all_to_all x1, waiting for transfers between devices, sum_at_owner(): parts = lax.all_to_all(in_blocks(x, dim, size), axis, 0, 0, tiled=True)  48.5 us
    all_gather x1, blocking collectives, turned_gather(): result = lax.all_gather(both, axis, axis=0, tiled=True)  29.8 us
    all_to_all x1, waiting for transfers between devices, shards(): lax.all_to_all(expert_out, 'ep', split_axis=1, concat_axis=1, tiled=True)  11.5 us
    all_to_all x1, starting transfers between devices, shards(): lax.all_to_all(expert_out, 'ep', split_axis=1, concat_axis=1, tiled=True)  9.2 us
    all_to_all x1, starting transfers between devices, sum_at_owner(): parts = lax.all_to_all(in_blocks(x, dim, size), axis, 0, 0, tiled=True)  8.22 us
    all_to_all x1, waiting for transfers between devices, copy_for_each(): lax.all_to_all(jnp.broadcast_to(x[None], (size, *x.shape)), axis, 0, 0, t...  6.95 us
    all_to_all x1, starting transfers between devices, copy_for_each(): lax.all_to_all(jnp.broadcast_to(x[None], (size, *x.shape)), axis, 0, 0, t...  6.42 us
  transfers between devices with their start and end apart: 3, of which 3 were waited for; matrix products, arithmetic and copies ran while one was open for 0% of the time, Pallas kernels for 0%

commit v1 on v0

v1 whole, which is shorter than its diff:
```python
import functools

import jax
import jax.numpy as jnp
from jax import lax
from jax.experimental import pallas as pl
from jax.experimental.pallas import tpu as pltpu
from jax.sharding import PartitionSpec as P

MESH = pl.DeviceIdType.MESH
F32 = jnp.float32
BF16 = jnp.bfloat16
epsilon = 1e-06

NZ, NY, NX = 8, 8, 8
EP, TP = NZ * NY, 2 * NX
CAP = 8
ROWS = EP * CAP
NC = 4
SC = EP // NC
RC = SC * CAP
FAR = NX // 2
HOP_ORDER = (4, 3, 5, 2, 6, 1, 7, 0)


def rank_offset(r):
    return ((r % 2) * ((r + 1) // 2) + (1 - r % 2) * (8 - r // 2)) % 8


def chunk(k):
    return pl.ds(k * SC, SC)


def kernel(
    tok_ref, gain_ref, routes_ref, gw_ref, wg_hbm, wu_hbm, wd_hbm, og_ref,
    out_ref,
    send_s, xg, gains, xs, ss, wg, wu, wd, own, ps, pr, sb_r, sb_l, rb_r, rb_l, eo, cb, g_hi, g_lo, hid, nb,
    w_sem, a_send, a_recv, gain_send, gain_recv,
    r_send, l_send, p_send, x_recv, p_recv,
    ps_send, pr_recv, rr_send, rl_send, rr_recv, rl_recv,
    b_send, b_recv, n_send, n_recv,
):
    ep = lax.axis_index("ep")
    tp = lax.axis_index("tp")
    z, y = ep // NY, ep % NY
    x, c = tp // 2, tp % 2
    right = (ep, ((x + 1) % NX) * 2 + c)
    left = (ep, ((x + NX - 1) % NX) * 2 + c)
    partner = (ep, x * 2 + 1 - c)

    def expert_of(o):
        return ((z + rank_offset(o // NY)) % NZ) * NY + (y + rank_offset(o % NY)) % NY

    def source_of(o):
        return ((z + NZ - rank_offset(o // NY)) % NZ) * NY + (y + NY - rank_offset(o % NY)) % NY

    barrier = pltpu.get_barrier_semaphore()

    def greet_ep(o, carry):
        pl.semaphore_signal(barrier, inc=1, device_id=(expert_of(o), tp), device_id_type=MESH)
        return carry

    def greet_tp(q, carry):
        pl.semaphore_signal(barrier, inc=1, device_id=(ep, (tp + q) % TP), device_id_type=MESH)
        return carry

    lax.fori_loop(1, EP, greet_ep, 0)
    lax.fori_loop(1, TP, greet_tp, 0)

    for d in range(NX):
        chip = (x + d) % NX
        for p in range(2):
            block = chip * 2 + (c if p == 0 else 1 - c)
            at = pl.multiple_of(block * 128, 128)
            to = pl.ds((2 * d + p) * 128, 128)
            pltpu.make_async_copy(wg_hbm.at[pl.ds(at, 128)], wg.at[to], w_sem.at[0]).start()
            pltpu.make_async_copy(wu_hbm.at[pl.ds(at, 128)], wu.at[to], w_sem.at[1]).start()
            pltpu.make_async_copy(wd_hbm.at[:, pl.ds(at, 128)], wd.at[:, to], w_sem.at[2]).start()

    row = lax.broadcasted_iota(jnp.int32, (ROWS, 128), 0)
    o = row >> 3
    a, b = o >> 3, o & 7

    def vec_offset(r):
        return jnp.where((r & 1) == 1, (r + 1) >> 1, (8 - (r >> 1)) & 7)

    expert = (((z + vec_offset(a)) & 7) << 3) + ((y + vec_offset(b)) & 7)
    is0 = expert == routes_ref[0:1, :]
    is1 = expert == routes_ref[1:2, :]
    named = jnp.where(is0 | is1, 1.0, 0.0)
    upper = jnp.where(
        lax.broadcasted_iota(jnp.int32, (128, 128), 0) < lax.broadcasted_iota(jnp.int32, (128, 128), 1), 1.0, 0.0
    ).astype(BF16)
    before = jnp.dot(named.astype(BF16), upper, preferred_element_type=F32)
    here = (before == (row & 7).astype(F32)) & (named > 0.5)
    scatter = jnp.where(here, 1.0, 0.0).astype(BF16)
    outgoing = jnp.dot(scatter, tok_ref[...], preferred_element_type=F32)
    send_s[...] = outgoing.reshape(EP, CAP, 128).astype(BF16)
    xg[0, 0, 0] = outgoing[0:CAP].astype(BF16)
    gates = jnp.where(here, jnp.where(is0, gw_ref[0:1, :], gw_ref[1:2, :]), 0.0)
    hi = gates.astype(BF16)
    g_hi[...] = hi
    g_lo[...] = (gates - hi.astype(F32)).astype(BF16)
    gains[0] = jnp.broadcast_to(gain_ref[...].astype(F32), (CAP, 128)).astype(BF16)

    pl.semaphore_wait(barrier, EP + TP - 2)

    def send_gain(q, carry):
        pltpu.make_async_remote_copy(
            src_ref=gains.at[0], dst_ref=gains.at[q], send_sem=gain_send, recv_sem=gain_recv,
            device_id=(ep, (tp + TP - q) % TP), device_id_type=MESH,
        ).start()
        return carry

    def send_row(k):
        def body(i, carry):
            pltpu.make_async_remote_copy(
                src_ref=send_s.at[i], dst_ref=xg.at[0, 0, i], send_sem=a_send, recv_sem=a_recv.at[k],
                device_id=(expert_of(i), tp), device_id_type=MESH,
            ).start()
            return carry
        return body

    for k in range(NC):
        lax.fori_loop(max(1, k * SC), (k + 1) * SC, send_row(k), 0)
    lax.fori_loop(1, TP, send_gain, 0)

    def r_copy(h, k):
        return pltpu.make_async_remote_copy(
            src_ref=xg.at[(NX - h) % NX, 0, chunk(k)], dst_ref=xg.at[NX - h - 1, 0, chunk(k)],
            send_sem=r_send.at[h, k], recv_sem=x_recv.at[NX - h - 1, k], device_id=right, device_id_type=MESH,
        )

    def l_copy(h, k):
        return pltpu.make_async_remote_copy(
            src_ref=xg.at[h, 0, chunk(k)], dst_ref=xg.at[h + 1, 0, chunk(k)],
            send_sem=l_send.at[h, k], recv_sem=x_recv.at[h + 1, k], device_id=left, device_id_type=MESH,
        )

    def p_copy(d, k):
        return pltpu.make_async_remote_copy(
            src_ref=xg.at[d, 0, chunk(k)], dst_ref=xg.at[d, 1, chunk(k)],
            send_sem=p_send.at[d, k], recv_sem=p_recv.at[d, k], device_id=partner, device_id_type=MESH,
        )

    def goes_right(h, k):
        return h < FAR - 1 or (h == FAR - 1 and k % 2 == 0)

    def goes_left(h, k):
        return h < FAR - 1 or (h == FAR - 1 and k % 2 == 1)

    def take_in(d, p, k):
        value = xg[d, p, chunk(k)].astype(F32).reshape(RC, 128)
        square = value * value
        rows = pl.ds(k * RC, RC)
        if d == 0 and p == 0:
            ss[rows] = square
        else:
            ss[rows] += square
        q = gains_slot(d, p)
        gain = gains[q].astype(F32)[0:1]
        xs[rows, pl.ds((2 * d + p) * 128, 128)] = (value * gain).astype(BF16)

    def take_both(d, k):
        take_in(d, 0, k)
        p_copy(d, k).wait_recv()
        take_in(d, 1, k)

    def gains_slot(d, p):
        return 2 * d if p == 0 else (2 * d + 1 + TP - 2 * c) % TP

    steps = sorted(
        ((h * 3.5 + k * 1.5, h, k) for h in range(FAR + 1) for k in range(NC))
    )
    pending, taken = [], []
    for _, h, k in steps:
        pending, taken = taken, []
        if h == 0:
            first = max(1, k * SC)
            got = xg.at[0, 0, pl.ds(first, (k + 1) * SC - first)]
            pltpu.make_async_copy(got, got, a_recv.at[k]).wait()
            r_copy(0, k).start()
            l_copy(0, k).start()
            p_copy(0, k).start()
            taken.append((0, k))
        elif h < FAR:
            r_copy(h - 1, k).wait_recv()
            if goes_right(h, k):
                r_copy(h, k).start()
            p_copy(NX - h, k).start()
            l_copy(h - 1, k).wait_recv()
            if goes_left(h, k):
                l_copy(h, k).start()
            p_copy(h, k).start()
            taken.append((NX - h, k))
            taken.append((h, k))
        else:
            (r_copy if goes_right(h - 1, k) else l_copy)(h - 1, k).wait_recv()
            p_copy(FAR, k).start()
            taken.append((FAR, k))
        if (h, k) == (0, 0):
            rest = gains.at[pl.ds(1, TP - 1)]
            pltpu.make_async_copy(rest, rest, gain_recv).wait()
        for item in pending:
            take_both(*item)
    for item in taken:
        take_both(*item)

    pltpu.make_async_copy(wg_hbm, wg, w_sem.at[0]).wait()
    pltpu.make_async_copy(wu_hbm, wu, w_sem.at[1]).wait()
    pltpu.make_async_copy(wd_hbm, wd, w_sem.at[2]).wait()
    scale = lax.rsqrt(jnp.sum(ss[...], axis=1, keepdims=True) * (1.0 / (128 * TP)) + epsilon)
    gate = jnp.dot(xs[...], wg[...], preferred_element_type=F32) * scale
    up = jnp.dot(xs[...], wu[...], preferred_element_type=F32) * scale
    hid[...] = (gate / (1.0 + jnp.exp(-gate)) * up).astype(BF16)

    def ps_copy(d):
        return pltpu.make_async_remote_copy(
            src_ref=ps.at[d], dst_ref=pr.at[d], send_sem=ps_send.at[d], recv_sem=pr_recv.at[d],
            device_id=partner, device_id_type=MESH,
        )

    for d in HOP_ORDER:
        part = jnp.dot(hid[...], wd[:, pl.ds(d * 256, 256)], preferred_element_type=F32)
        ps[d] = part[:, 128:256].reshape(EP, CAP, 128).astype(BF16)
        ps_copy(d).start()
        own[d] = part[:, 0:128]

    def rr_copy(j, k):
        return pltpu.make_async_remote_copy(
            src_ref=sb_r.at[j, chunk(k)], dst_ref=rb_r.at[j, chunk(k)],
            send_sem=rr_send.at[j, k], recv_sem=rr_recv.at[j, k], device_id=right, device_id_type=MESH,
        )

    def rl_copy(j, k):
        return pltpu.make_async_remote_copy(
            src_ref=sb_l.at[j, chunk(k)], dst_ref=rb_l.at[j, chunk(k)],
            send_sem=rl_send.at[j, k], recv_sem=rl_recv.at[j, k], device_id=left, device_id_type=MESH,
        )

    def chip_part(d, k):
        return own[d, pl.ds(k * RC, RC)] + pr[d, chunk(k)].astype(F32).reshape(RC, 128)

    def has(j, k, side):
        return j > 0 or k % 2 == side

    def b_copy(i):
        return pltpu.make_async_remote_copy(
            src_ref=eo.at[i], dst_ref=cb.at[i], send_sem=b_send, recv_sem=b_recv,
            device_id=(source_of(i), tp), device_id_type=MESH,
        )

    def send_back(i, carry):
        b_copy(i).start()
        return carry

    for d in HOP_ORDER:
        ps_copy(d).wait_recv()

    order = tuple(reversed(range(NC)))
    steps = sorted((j * 3.5 + n * 1.0, j, k) for j in range(FAR + 1) for n, k in enumerate(order))
    for _, j, k in steps:
        if j < FAR:
            for side, copy, sb, rb, d in (
                (0, rr_copy, sb_r, rb_r, FAR - j),
                (1, rl_copy, sb_l, rb_l, (FAR + j) % NX),
            ):
                if not has(j, k, side):
                    continue
                total = chip_part(d, k)
                if j > 0 and has(j - 1, k, side):
                    copy(j - 1, k).wait_recv()
                    total = total + rb[j - 1, chunk(k)].astype(F32).reshape(RC, 128)
                sb[j, chunk(k)] = total.reshape(SC, CAP, 128).astype(BF16)
                copy(j, k).start()
        else:
            rr_copy(FAR - 1, k).wait_recv()
            rl_copy(FAR - 1, k).wait_recv()
            total = (
                chip_part(0, k)
                + rb_r[FAR - 1, chunk(k)].astype(F32).reshape(RC, 128)
                + rb_l[FAR - 1, chunk(k)].astype(F32).reshape(RC, 128)
            )
            result = total.reshape(SC, CAP, 128).astype(BF16)
            eo[chunk(k)] = result
            if k == 0:
                cb[0] = result[0]
            lax.fori_loop(max(1, k * SC), (k + 1) * SC, send_back, 0)

    rest = cb.at[pl.ds(1, EP - 1)]
    pltpu.make_async_copy(rest, rest, b_recv).wait()
    back = cb[...].astype(F32).reshape(ROWS, 128).astype(BF16)
    across = (((0,), (0,)), ((), ()))
    combined = lax.dot_general(g_hi[...], back, across, preferred_element_type=F32) + lax.dot_general(
        g_lo[...], back, across, preferred_element_type=F32
    )

    eye = lax.broadcasted_iota(jnp.int32, (128, 128), 0) == lax.broadcasted_iota(jnp.int32, (128, 128), 1)
    column = jnp.sum(combined * combined, axis=1, keepdims=True)
    line = jnp.sum(jnp.where(eye, column, 0.0), axis=0, keepdims=True)
    nb[0] = jnp.broadcast_to(line, (8, 128))

    def n_copy(q):
        return pltpu.make_async_remote_copy(
            src_ref=nb.at[0], dst_ref=nb.at[q], send_sem=n_send, recv_sem=n_recv,
            device_id=(ep, (tp + q) % TP), device_id_type=MESH,
        )

    def send_norm(q, carry):
        n_copy(q).start()
        return carry

    lax.fori_loop(1, TP, send_norm, 0)
    rest = nb.at[pl.ds(1, TP - 1)]
    pltpu.make_async_copy(rest, rest, n_recv).wait()
    total = jnp.sum(nb[...], axis=0)[0:1]
    scale_line = lax.rsqrt(total * (1.0 / (128 * TP)) + epsilon)
    scale_out = jnp.sum(jnp.where(eye, scale_line, 0.0), axis=1, keepdims=True)
    out_ref[...] = (combined * scale_out * og_ref[...].astype(F32)).astype(BF16)

    pltpu.make_async_copy(rest, rest, n_send).wait()
    sent = send_s.at[pl.ds(1, EP - 1)]
    pltpu.make_async_copy(sent, sent, a_send).wait()
    sent = eo.at[pl.ds(1, EP - 1)]
    pltpu.make_async_copy(sent, sent, b_send).wait()
    sent = gains.at[pl.ds(1, TP - 1)]
    pltpu.make_async_copy(sent, sent, gain_send).wait()
    for k in range(NC):
        for h in range(FAR):
            if goes_right(h, k):
                r_copy(h, k).wait_send()
            if goes_left(h, k):
                l_copy(h, k).wait_send()
        for d in range(NX):
            p_copy(d, k).wait_send()
        for j in range(FAR):
            if has(j, k, 0):
                rr_copy(j, k).wait_send()
            if has(j, k, 1):
                rl_copy(j, k).wait_send()
    for d in range(NX):
        ps_copy(d).wait_send()


def shards(tokens, norm_gain, routes, gate_weights, w_gate, w_up, w_down, out_gain):
    vmem = pl.BlockSpec(memory_space=pltpu.VMEM)
    hbm = pl.BlockSpec(memory_space=pl.ANY)
    dma = pltpu.SemaphoreType.DMA
    width = tokens.shape[1]
    features = width * TP
    units = w_gate.shape[2]
    return pl.pallas_call(
        kernel,
        out_shape=jax.ShapeDtypeStruct(tokens.shape, BF16),
        in_specs=[vmem, vmem, vmem, vmem, hbm, hbm, hbm, vmem],
        out_specs=vmem,
        scratch_shapes=[
            pltpu.VMEM((EP, CAP, width), BF16),
            pltpu.VMEM((NX, 2, EP, CAP, width), BF16),
            pltpu.VMEM((TP, CAP, width), BF16),
            pltpu.VMEM((ROWS, features), BF16),
            pltpu.VMEM((ROWS, width), F32),
            pltpu.VMEM((features, units), BF16),
            pltpu.VMEM((features, units), BF16),
            pltpu.VMEM((units, features), BF16),
            pltpu.VMEM((NX, ROWS, width), F32),
            pltpu.VMEM((NX, EP, CAP, width), BF16),
            pltpu.VMEM((NX, EP, CAP, width), BF16),
            pltpu.VMEM((FAR, EP, CAP, width), BF16),
            pltpu.VMEM((FAR, EP, CAP, width), BF16),
            pltpu.VMEM((FAR, EP, CAP, width), BF16),
            pltpu.VMEM((FAR, EP, CAP, width), BF16),
            pltpu.VMEM((EP, CAP, width), BF16),
            pltpu.VMEM((EP, CAP, width), BF16),
            pltpu.VMEM((ROWS, 128), BF16),
            pltpu.VMEM((ROWS, 128), BF16),
            pltpu.VMEM((ROWS, units), BF16),
            pltpu.VMEM((TP, 8, 128), F32),
            dma((3,)), dma, dma((NC,)), dma, dma,
            dma((FAR, NC)), dma((FAR, NC)), dma((NX, NC)), dma((NX, NC)), dma((NX, NC)),
            dma((NX,)), dma((NX,)), dma((FAR, NC)), dma((FAR, NC)), dma((FAR, NC)), dma((FAR, NC)),
            dma, dma, dma, dma,
        ],
        compiler_params=pltpu.CompilerParams(
            collective_id=0, has_side_effects=True, vmem_limit_bytes=60 * 1024 * 1024
        ),
        name="layer",
    )(
        tokens, norm_gain.reshape(1, -1), routes.T, gate_weights.T, w_gate[0], w_up[0], w_down[0],
        out_gain.reshape(1, -1),
    )


def solution(mesh):
    placed = (
        P("ep", "tp"),
        P("tp"),
        P("ep", None),
        P("ep", None),
        P("ep", None, "tp"),
        P("ep", None, "tp"),
        P("ep", "tp", None),
        P("tp"),
    )
    return jax.shard_map(
        shards, mesh=mesh, in_specs=placed, out_specs=P("ep", "tp"), check_vma=False
    )
```

time: 203 us -> 88.4 us (0.44)
  blocking collectives: 92.9 us -> 0 us
  Pallas kernels: 0 us -> 86.7 us
  waiting for transfers between devices: 67 us -> 0 us
  starting transfers between devices: 23.8 us -> 0 us
  matrix products: 7.33 us -> 0 us
  local copies, waits for them, and re-layouts: 6.96 us -> 1.38 us
  other arithmetic: 4.66 us -> 0 us
    pallas_call x0 -> x1, Pallas kernels: none -> 86.7 us  [shards(): pl.pallas_call(kernel, out_shape=jax.ShapeDtypeStruct(tokens.shape, BF16)...]
    all_to_all x3 -> x0, waiting for transfers between devices: 67 us -> none  [the longest x1 48.5 us: sum_at_owner(): parts = lax.all_to_all(in_blocks(x, dim, size), axis, 0, 0, tiled=True)]
    all_to_all x1 -> x0, blocking collectives: 63.1 us -> none  [shards(): lax.all_to_all(outgoing, 'ep', split_axis=0, concat_axis=0, tiled=True)]
    all_gather x1 -> x0, blocking collectives: 29.8 us -> none  [turned_gather(): result = lax.all_gather(both, axis, axis=0, tiled=True)]
    all_to_all x3 -> x0, starting transfers between devices: 23.8 us -> none  [the longest x1 9.2 us: shards(): lax.all_to_all(expert_out, 'ep', split_axis=1, concat_axis=1, tiled=True)]
    dot_general x3 -> x0, matrix products: 7.33 us -> none  [the longest x1 5.02 us: shards(): lax.dot_general(down_mat, hidden, (((0,), (1,)), ((), ())), preferred_ele...]
    reshape x2 -> x0, local copies, waits for them, and re-layouts: 3.57 us -> none  [the longest x1 3.43 us: in_blocks(): x.reshape(*lengths[:dim], size, lengths[dim] // size, *lengths[dim + 1:])]
  transfers between devices with their start and end apart: 3 -> 0, of which waited for: 3 -> 0; matrix products, arithmetic and copies ran while one was open for 0% -> 0% of each run, Pallas kernels for 0% -> 0%
where the time goes in v1:
time: 88.4 us; the launch traced here: 88.1 us
  Pallas kernels  86.7 us (98%)
  local copies, waits for them, and re-layouts  1.38 us (2%)
    pallas_call x1, Pallas kernels, shards(): pl.pallas_call(kernel, out_shape=jax.ShapeDtypeStruct(tokens.shape, BF16)...  86.7 us

profile of v1, /device:TPU:1, one launch (start us, length us, event | category | flops | bytes accessed | tf_op | source)
XLA Modules:
  0.0 88.1 jit_solution(936927746908523864)
XLA Ops:
  0.0 86.7 %layer.1 = bf16[128,128]{1,0:T(8,128)(2,1)} custom-call(bf16[128,128]{1,0:T(8,128)(2,1)} %tok_ref.1, bf16[1,128]{1,0:T(2,128)(2,1)} %bitcast.12, s32[2,128]{1,0:T(2,128)} %bitcast.10, f32[2,128]{1,0:T(2,128)} %bitcast.11, bf16[2048,256]{1,0:T(8,128)(2,1)} %bitcast.7, bf16[2048,256]{1,0:T(8,128)(2,1)} %bitcast.8, bf16[256,2048]{1,0:T(8,128)(2,1)} %bitcast.9, ...), custom_call_target="tpu_custom_call" | custom-call | tf_op jit(solution)/shard_map/layer/pallas_call | solution.py:352
  86.7 1.4 %copy.10 = bf16[128,128]{1,0:T(8,128)(2,1)} copy(bf16[128,128]{1,0:T(8,128)(2,1)} %layer.1) | data formatting | bytes 65536
